TPU v7x, 32 devices: a whole 2x2x4 slice. The times are simulated.
32 devices in a mesh: ep: 32 (over z, y, x, core).
Axes of the slice: x: 2, y: 2, z: 4, core: 2. Of those that a mesh axis runs over, the one named last changes fastest.
Arguments:
- tokens: bfloat16 [576, 2048], P('ep'), may hold values from -6 to 6
- attn_norm_gain: float32 [2048], replicated, may hold values from 0.1 to 1.9
- w_query: bfloat16 [2048, 512], replicated, may hold values from -0.125 to 0.125
- w_key: bfloat16 [2048, 128], replicated, may hold values from -0.125 to 0.125
- w_value: bfloat16 [2048, 128], replicated, may hold values from -0.125 to 0.125
- w_forget: bfloat16 [2048, 8], replicated, may hold values from -0.125 to 0.125
- forget_bias: float32 [8], replicated, may hold values from 0.5 to 4
- w_attn_out: bfloat16 [512, 2048], replicated, may hold values from -0.25 to 0.25
- cache_keys: bfloat16 [576, 1024, 128], P('ep'), may hold values from -72 to 72
- cache_values: bfloat16 [576, 1024, 128], P('ep'), may hold values from -6 to 6
- cache_logcum: float32 [576, 8, 1024], P('ep'), as said below
- cache_lengths: int32 [576], P('ep'), may hold values from 128 to 1024
- expert_norm_gain: float32 [2048], replicated, may hold values from 0.4 to 40
- expert_ids: int32 [576, 6], P('ep'), may hold values from 0 to 31, all different within a row; in each aligned block of 18 rows (0 to 17, 18 to 35, ...) at most 6 rows name the same one
- expert_weights: float32 [576, 6], P('ep'), may hold values from 0.1 to 1
- w_expert_gate: bfloat16 [32, 2048, 512], P('ep'), may hold values from -0.125 to 0.125
- w_expert_up: bfloat16 [32, 2048, 512], P('ep'), may hold values from -0.125 to 0.125
- w_expert_down: bfloat16 [32, 512, 2048], P('ep'), may hold values from -0.25 to 0.25
- w_dense_gate: bfloat16 [2048, 4096], P(None, 'ep'), may hold values from -0.125 to 0.125
- w_dense_up: bfloat16 [2048, 4096], P(None, 'ep'), may hold values from -2 to 2
- w_dense_down: bfloat16 [4096, 2048], P('ep'), may hold values from -0.09375 to 0.09375
- dense_norm_gain: float32 [4096], replicated, may hold values from 0.1 to 1.9
- branch_gate: float32 [2048], replicated, may hold values from -0.125 to 0.125
Outputs:
- result: bfloat16 [576, 2048], P('ep')
Inputs may be any that keep to these rules, and one draw needn't show every extreme that they name: `cache_logcum`: along the positions of each sequence and head the values never rise. `expert_ids`: each row names 6 different experts; among the rows of one device no expert is named by more than 6 rows, and in every draw some device names some expert exactly 6 times.
All inputs are finite; a program needn't handle non-finite values.
Results may differ from a plain program's by a relative error of at most 0.012.
The roundings to bfloat16 on the way count: a program that leaves them out, or rounds other values in their place, can miss the bound.
Values may be sent and summed in bfloat16 or wider, within the bound.
A program may use at most 128 MiB of HBM per device.

v0:
```python
import jax
import jax.numpy as jnp
from jax import lax
from jax.sharding import PartitionSpec as P

HEADS = 8
KV_HEADS = 2
HEAD_DIM = 64
TOPK = 6


EPS = 1e-06
LIMIT = 7.0
ALPHA = 1.702


def normalize(values, gain):
    return values * lax.rsqrt(jnp.mean(values * values, axis=-1, keepdims=True) + EPS) * gain


def stored(values):
    return lax.optimization_barrier(values.astype(jnp.bfloat16))


def attend(
    query, key_new, value_new, log_forget, cache_keys, cache_values, cache_logcum, cache_lengths
):
    seqs, length = (cache_keys.shape[0], cache_keys.shape[1])
    group = HEADS // KV_HEADS
    scale = HEAD_DIM ** (-0.5)
    heads_q = query.reshape(seqs, KV_HEADS, group, HEAD_DIM)
    keys = cache_keys.reshape(seqs, length, KV_HEADS, HEAD_DIM)
    values = cache_values.reshape(seqs, length, KV_HEADS, HEAD_DIM)
    own_key = key_new.reshape(seqs, KV_HEADS, HEAD_DIM)
    own_value = value_new.astype(jnp.float32).reshape(seqs, KV_HEADS, 1, HEAD_DIM)
    last_index = jnp.broadcast_to((cache_lengths - 1)[:, None, None], (seqs, HEADS, 1))
    carried = jnp.take_along_axis(cache_logcum, last_index, axis=2)[:, :, 0] + log_forget
    offset = (carried[:, :, None] - cache_logcum).reshape(seqs, KV_HEADS, group, length)
    scores = (
        jnp.einsum("skgd,slkd->skgl", heads_q, keys, preferred_element_type=jnp.float32) * scale
        + offset
    )
    live = jnp.arange(length, dtype=jnp.int32)[None, :] < cache_lengths[:, None]
    scores = jnp.where(live[:, None, None, :], scores, -jnp.inf)
    own = jnp.einsum("skgd,skd->skg", heads_q, own_key, preferred_element_type=jnp.float32) * scale
    top = jnp.maximum(jnp.max(scores, axis=-1), own)
    expo = jnp.exp(scores - top[..., None])
    own_expo = jnp.exp(own - top)
    total = jnp.sum(expo, axis=-1) + own_expo
    weights = (expo / total[..., None]).astype(jnp.bfloat16)
    own_weight = stored(own_expo / total).astype(jnp.float32)
    out = jnp.einsum("skgl,slkd->skgd", weights, values, preferred_element_type=jnp.float32)
    out = out + own_weight[..., None] * own_value
    return out.reshape(seqs, HEADS * HEAD_DIM).astype(jnp.bfloat16)


def expert_unit(rows, gate_w, up_w, down_w):
    gate = jnp.minimum(jnp.dot(rows, gate_w, preferred_element_type=jnp.float32), LIMIT)
    up = jnp.clip(jnp.dot(rows, up_w, preferred_element_type=jnp.float32), -LIMIT, LIMIT)
    act = ((up + 1.0) * gate * jax.nn.sigmoid(gate * ALPHA)).astype(jnp.bfloat16)
    return jnp.dot(act, down_w, preferred_element_type=jnp.float32).astype(jnp.bfloat16)


def shards(
    tokens,
    attn_norm_gain,
    w_query,
    w_key,
    w_value,
    w_forget,
    forget_bias,
    w_attn_out,
    cache_keys,
    cache_values,
    cache_logcum,
    cache_lengths,
    expert_norm_gain,
    expert_ids,
    expert_weights,
    w_expert_gate,
    w_expert_up,
    w_expert_down,
    w_dense_gate,
    w_dense_up,
    w_dense_down,
    dense_norm_gain,
    branch_gate,
):
    seqs, width = (tokens.shape[0], tokens.shape[1])
    normed = normalize(tokens.astype(jnp.float32), attn_norm_gain).astype(jnp.bfloat16)
    query = jnp.dot(normed, w_query, preferred_element_type=jnp.float32).astype(jnp.bfloat16)
    key_new = jnp.dot(normed, w_key, preferred_element_type=jnp.float32).astype(jnp.bfloat16)
    value_new = jnp.dot(normed, w_value, preferred_element_type=jnp.float32).astype(jnp.bfloat16)
    log_forget = jax.nn.log_sigmoid(
        jnp.dot(normed, w_forget, preferred_element_type=jnp.float32) + forget_bias
    )
    attended = attend(
        query, key_new, value_new, log_forget, cache_keys, cache_values, cache_logcum, cache_lengths
    )
    mixed = stored(
        tokens.astype(jnp.float32)
        + jnp.dot(attended, w_attn_out, preferred_element_type=jnp.float32)
    )
    routed_in = normalize(mixed.astype(jnp.float32), expert_norm_gain).astype(jnp.bfloat16)
    devices = lax.axis_size("ep")
    experts = devices * w_expert_gate.shape[0]
    capacity = max(2, 2 * seqs * TOPK // experts)
    flat_ids = expert_ids.reshape(-1)
    member = (flat_ids[:, None] == jnp.arange(experts, dtype=jnp.int32)[None, :]).astype(jnp.int32)
    slot = jnp.sum(jnp.cumsum(member, axis=0) * member, axis=1) - 1
    target = flat_ids * capacity + slot
    placement = (
        target[:, None] == jnp.arange(experts * capacity, dtype=jnp.int32)[None, :]
    ).astype(jnp.float32)
    per_token = jnp.sum(placement.reshape(seqs, TOPK, experts * capacity), axis=1).astype(
        jnp.bfloat16
    )
    outgoing = jnp.einsum("sc,sd->cd", per_token, routed_in, preferred_element_type=jnp.float32)
    outgoing = outgoing.astype(jnp.bfloat16).reshape(experts, capacity, width)
    arrived = lax.all_to_all(outgoing, "ep", split_axis=0, concat_axis=0, tiled=True)
    count = arrived.shape[1]
    answer = expert_unit(
        arrived.reshape(-1, width), w_expert_gate[0], w_expert_up[0], w_expert_down[0]
    )
    returned = lax.all_to_all(
        answer.reshape(devices, count, width), "ep", split_axis=0, concat_axis=0, tiled=True
    )
    picked = jnp.dot(
        placement.astype(jnp.bfloat16),
        returned.reshape(experts * capacity, width),
        preferred_element_type=jnp.float32,
    )
    routed = jnp.sum(expert_weights[:, :, None] * picked.reshape(seqs, TOPK, width), axis=1)
    piece = lax.all_gather(routed_in, "ep", axis=0, tiled=True)
    gate_dense = jnp.dot(piece, w_dense_gate, preferred_element_type=jnp.float32)
    up_dense = jnp.dot(piece, w_dense_up, preferred_element_type=jnp.float32)
    units = (jax.nn.silu(gate_dense) * up_dense).astype(jnp.bfloat16)
    own_units = lax.all_to_all(units, "ep", split_axis=0, concat_axis=1, tiled=True).astype(
        jnp.float32
    )
    unit_scale = lax.rsqrt(jnp.mean(own_units * own_units, axis=1, keepdims=True) + EPS)
    hidden = (own_units * unit_scale * dense_norm_gain).astype(jnp.bfloat16)
    dense = jnp.dot(
        hidden,
        lax.all_gather(w_dense_down, "ep", axis=0, tiled=True),
        preferred_element_type=jnp.float32,
    )
    branch_scale = jax.nn.sigmoid(
        jnp.sum(routed_in.astype(jnp.float32) * branch_gate, axis=1, keepdims=True)
    )
    return (mixed.astype(jnp.float32) + routed + branch_scale * dense).astype(jnp.bfloat16)


def solution(mesh):
    in_specs = (
        P("ep", None),
        P(),
        P(),
        P(),
        P(),
        P(),
        P(),
        P(),
        P("ep", None, None),
        P("ep", None, None),
        P("ep", None, None),
        P("ep"),
        P(),
        P("ep", None),
        P("ep", None),
        P("ep", None, None),
        P("ep", None, None),
        P("ep", None, None),
        P(None, "ep"),
        P(None, "ep"),
        P("ep", None),
        P(),
        P(),
    )
    out_specs = P("ep", None)
    return jax.shard_map(shards, mesh=mesh, in_specs=in_specs, out_specs=out_specs, check_vma=False)
```

profile of v0, /device:TPU:0, one launch (start us, length us, event | category | flops | bytes accessed | tf_op | source)
XLA Modules:
  0.0 255.5 jit_solution(114577591196382522)
XLA Ops:
  6.5 0.8 broadcast_add_fusion.1
  7.3 0.7 broadcast_compare_fusion
  8.0 0.7 iota_compare_fusion.2
  9.0 5.5 %gather_fusion = f32[144]{0:T(256)S(1)} fusion(f32[18,8,1024]{2,1,0:T(8,128)} %param.33, s32[144]{0:T(256)S(1)} %reshape.290), kind=kCustom, calls=%fused_computation | custom fusion | bytes 2880 | tf_op jit(solution)/shard_map/jit(take_along_axis)/gather | solution.py:37
  14.7 0.1 fusion.44
  14.9 0.2 fusion.62
  15.2 0.9 broadcast_subtract_fusion
  16.2 1.2 reshape.279
  17.4 2.0 convolution_convert_fusion.2
  19.4 0.1 reshape.277
  19.5 6.7 %copy.47 = bf16[18,1024,128]{1,2,0:T(8,128)(2,1)} copy(bf16[18,1024,128]{2,1,0:T(8,128)(2,1)} %param.31) | data formatting | bytes 9437184 | tf_op args[8]
  26.2 0.2 convolution_convert_fusion.4
  26.6 0.2 fusion.81
  26.7 3.3 %fusion.80 = (f32[18,2,4]{2,1,0:T(2,128)S(1)}, f32[18,2,4,1024]{3,2,1,0:T(4,128)S(1)}) fusion(f32[18,2,4,1024]{3,2,1,0:T(4,128)S(1)} %reshape.279, bf16[18,2,4,64]{3,2,1,0:T(4,128)(2,1)S(1)} %reshape.277, bf16[18,1024,2,64]{1,3,2,0:T(8,128)(2,1)} %bitcast.61, pred[18,1024]{1,0:T(8,128)(4,1)S(1)} %iota_compare_fusion.2), kind=kOutput, calls=%fused_computation.112 | convolution fusion | flops 19464048 | bytes 5935680 | tf_op jit(solution)/shard_map/skgd,slkd->skgl/dot_general | solution.py:40
  30.1 0.4 fusion.35
  30.5 0.2 fusion.33
  30.8 6.6 %copy.51 = bf16[18,1024,128]{1,2,0:T(8,128)(2,1)} copy(bf16[18,1024,128]{2,1,0:T(8,128)(2,1)} %param.32) | data formatting | bytes 9437184 | tf_op args[9]
  37.5 3.7 %fusion.32 = bf16[18,2,4,64]{3,2,1,0:T(4,128)(2,1)S(1)} fusion(bf16[18,1024,2,64]{1,3,2,0:T(8,128)(2,1)} %bitcast.62, f32[18,2,4,1024]{3,2,1,0:T(4,128)S(1)} %get-tuple-element.12, f32[18,2,4]{2,1,0:T(2,128)S(1)} %get-tuple-element.8, f32[18,2,4]{2,1,0:T(2,128)S(1)} %multiply_maximum_fusion, f32[18,2,64]{2,1,0:T(2,128)S(1)} %reshape.286, ...), kind=kOutput, calls=%fused_computation.27 | convolution fusion | flops 19344384 | bytes 5337792 | tf_op jit(solution)/shard_map/skgl,slkd->skgd/dot_general | solution.py:52
  41.2 0.1 convert_element_type.130
  41.3 2.0 fusion.1
  43.3 0.1 fusion.47
  43.5 0.9 multiply_reduce_fusion
  44.4 0.7 all-gather.4.cloned.1.call-update
  45.4 0.2 reduce_window_sum.11
  45.5 0.2 select_reduce_fusion
  45.8 0.1 convert_reduce_fusion
  46.0 1.3 convolution_convert_fusion.1
  47.3 1.3 reshape.282
  48.6 37.9 %all_to_all.23 = bf16[32,6,2048]{2,1,0:T(8,128)(2,1)} all-to-all(bf16[32,6,2048]{2,1,0:T(8,128)(2,1)S(1)} %reshape.282), channel_id=1, replica_groups=mesh['ep'=32] {'ep'}, dimensions={0} | all-to-all | bytes 1572864 | tf_op jit(solution)/shard_map/all_to_all | solution.py:120
  86.5 1.4 reshape.283
  87.9 2.9 %fusion.23 = f32[192,512]{1,0:T(8,128)} fusion(bf16[192,2048]{1,0:T(8,128)(2,1)S(1)} %reshape.283, bf16[1,2048,512]{2,1,0:T(8,128)(2,1)} %param.38), kind=kOutput, calls=%fused_computation.22 | convolution fusion | flops 402751488 | bytes 3276800 | tf_op jit(solution)/shard_map/dot_general | solution.py:58
  90.8 3.6 %convolution_convert_fusion = bf16[192,2048]{1,0:T(8,128)(2,1)} fusion(bf16[1,512,2048]{2,1,0:T(8,128)(2,1)S(1)} %copy-done, f32[192,512]{1,0:T(8,128)} %fusion.23, bf16[192,2048]{1,0:T(8,128)(2,1)S(1)} %reshape.283, bf16[1,2048,512]{2,1,0:T(8,128)(2,1)} %param.39), kind=kOutput, calls=%fused_computation.2 | convolution fusion | flops 806584320 | bytes 6160384 | tf_op jit(solution)/shard_map/dot_general | solution.py:61
  94.4 2.2 reshape.284
  96.7 3.5 %all-to-all-start.1 = ((bf16[32,6,2048]{2,1,0:T(8,128)(2,1)}), bf16[32,6,2048]{2,1,0:T(8,128)(2,1)S(1)}, u32[]{:S(2)}, u32[]{:S(2)}) async-start(bf16[32,6,2048]{2,1,0:T(8,128)(2,1)} %reshape.284), calls=%async_computation.1 | async-start | bytes 2097152 | tf_op jit(solution)/shard_map/all_to_all | solution.py:125
  100.3 18.4 %all-gather.6.cloned.1.call-done = bf16[32,18,2048]{2,1,0:T(8,128)(2,1)} async-done(((bf16[1,18,2048]{2,1,0:T(8,128)(2,1)}), bf16[32,18,2048]{2,1,0:T(8,128)(2,1)}) %all-gather.6.cloned.1.call-update) | async-done | bytes 2359312 | tf_op jit(solution)/shard_map/all_gather | solution.py:134
  118.7 4.3 %reshape.299 = bf16[576,2048]{1,0:T(8,128)(2,1)} reshape(bf16[32,18,2048]{2,1,0:T(8,128)(2,1)} %all-gather.6.cloned.1.call-done) | data formatting | bytes 4718592
  123.1 2.6 %fusion.82 = f32[576,128]{1,0:T(8,128)S(1)} fusion(bf16[576,2048]{1,0:T(8,128)(2,1)} %reshape.299, bf16[2048,128]{1,0:T(8,128)(2,1)S(1)} %copy-done.5), kind=kOutput, calls=%fused_computation.114 | convolution fusion | flops 301989888 | bytes 3178496 | tf_op jit(solution)/shard_map/dot_general | solution.py:135
  125.7 0.8 fusion.29
  126.5 0.7 all_to_all.18
  127.2 4.0 %all-to-all-done.1 = bf16[32,6,2048]{2,1,0:T(8,128)(2,1)S(1)} async-done(((bf16[32,6,2048]{2,1,0:T(8,128)(2,1)}), bf16[32,6,2048]{2,1,0:T(8,128)(2,1)S(1)}, u32[]{:S(2)}, u32[]{:S(2)}) %all-to-all-start.1) | async-done | bytes 786464 | tf_op jit(solution)/shard_map/all_to_all | solution.py:125
  131.1 3.8 %all-to-all-start.2 = ((bf16[32,18,128]{2,1,0:T(8,128)(2,1)}), bf16[32,18,128]{2,1,0:T(8,128)(2,1)S(1)}, u32[]{:S(2)}, u32[]{:S(2)}) async-start(bf16[32,18,128]{2,1,0:T(8,128)(2,1)} %all_to_all.18), calls=%async_computation.2 | async-start | bytes 393216 | tf_op jit(solution)/shard_map/all_to_all | solution.py:138
  135.0 0.3 reshape.302
  135.2 0.6 fusion.8
  135.9 12.2 %all-to-all-done.2 = bf16[32,18,128]{2,1,0:T(8,128)(2,1)S(1)} async-done(((bf16[32,18,128]{2,1,0:T(8,128)(2,1)}), bf16[32,18,128]{2,1,0:T(8,128)(2,1)S(1)}, u32[]{:S(2)}, u32[]{:S(2)}) %all-to-all-start.2) | async-done | bytes 147488 | tf_op jit(solution)/shard_map/all_to_all | solution.py:138
  148.2 0.2 copy.58
  148.4 0.2 fusion.36
  148.6 91.2 %all-gather.4.cloned.1.call-done = bf16[4096,2048]{1,0:T(8,128)(2,1)} async-done(((bf16[128,2048]{1,0:T(8,128)(2,1)}), bf16[4096,2048]{1,0:T(8,128)(2,1)}) %all-gather.4.cloned.1.call-update) | async-done | bytes 16777232 | tf_op jit(solution)/shard_map/all_gather | solution.py:145
  239.8 8.9 %fusion.2 = bf16[18,2048]{1,0:T(8,128)(2,1)} fusion(bf16[4096,2048]{1,0:T(8,128)(2,1)} %all-gather.4.cloned.1.call-done, f32[18,2048]{1,0:T(8,128)S(1)} %fusion.8, bf16[18,2048]{1,0:T(8,128)(2,1)S(1)} %fusion.1, f32[18,4096]{1,0:T(8,128)S(1)} %bitcast.63, f32[4096]{0:T(1024)S(1)} %copy-done.9, f32[18]{0:T(128)S(1)} %add_rsqrt_fusion, f32[18]{0:T(128)S(1)} %add_divide_fusion), kind=kOutput, calls=%fused_computation.8 | convolution fusion | flops 302395392 | bytes 17383568 | tf_op jit(solution)/shard_map/dot_general | solution.py:143
  (66 shorter events, 1.4 us)
Async XLA Ops:
  6.5 84.3 %copy-start = (bf16[1,512,2048]{2,1,0:T(8,128)(2,1)S(1)}, bf16[1,512,2048]{2,1,0:T(8,128)(2,1)}, u32[]{:S(2)}) copy-start(bf16[1,512,2048]{2,1,0:T(8,128)(2,1)} %param.40) | copy-start | bytes 6291460
  6.5 112.2 %all-gather.6.cloned.1.call-start = ((), (), s32[]{:S(2)}) async-start(), calls=%async_computation.4 | async-start | bytes 3244032 | tf_op jit(solution)/shard_map/all_gather | solution.py:134
  9.0 5.7 %copy-start.4 = (bf16[18,2048]{1,0:T(8,128)(2,1)S(1)}, bf16[18,2048]{1,0:T(8,128)(2,1)}, u32[]{:S(2)}) copy-start(bf16[18,2048]{1,0:T(8,128)(2,1)} %param.23) | copy-start | bytes 221188
  9.0 5.9 %copy-start.8 = (f32[2048]{0:T(1024)S(1)}, f32[2048]{0:T(1024)}, u32[]{:S(2)}) copy-start(f32[2048]{0:T(1024)} %param.24) | copy-start | bytes 24580
  9.0 5.9 %copy-start.15 = (bf16[2048,8]{0,1:T(8,128)(2,1)S(1)}, bf16[2048,8]{0,1:T(8,128)(2,1)}, u32[]{:S(2)}) copy-start(bf16[2048,8]{0,1:T(8,128)(2,1)} %param.28) | copy-start | bytes 98308
  9.0 5.9 %copy-start.16 = (f32[8]{0:T(128)S(1)}, f32[8]{0:T(128)}, u32[]{:S(2)}) copy-start(f32[8]{0:T(128)} %param.29) | copy-start | bytes 100
  9.0 6.2 %copy-start.2 = (f32[18,8,1024]{2,1,0:T(8,128)S(1)}, f32[18,8,1024]{2,1,0:T(8,128)}, u32[]{:S(2)}) copy-start(f32[18,8,1024]{2,1,0:T(8,128)} %param.33) | copy-start | bytes 1769476
  19.5 6.7 %copy-start.6 = (bf16[2048,128]{1,0:T(8,128)(2,1)S(1)}, bf16[2048,128]{1,0:T(8,128)(2,1)}, u32[]{:S(2)}) copy-start(bf16[2048,128]{1,0:T(8,128)(2,1)} %param.26) | copy-start | bytes 1572868
  26.7 3.7 %copy-start.7 = (bf16[2048,128]{1,0:T(8,128)(2,1)S(1)}, bf16[2048,128]{1,0:T(8,128)(2,1)}, u32[]{:S(2)}) copy-start(bf16[2048,128]{1,0:T(8,128)(2,1)} %param.27) | copy-start | bytes 1572868
  41.2 2.3 copy-start.10
  41.2 2.3 copy-start.11
  41.2 3.9 %copy-start.12 = (s32[18,6]{0,1:T(8,128)S(1)}, s32[18,6]{0,1:T(8,128)}, u32[]{:S(2)}) copy-start(s32[18,6]{0,1:T(8,128)} %param.36) | copy-start | bytes 1300
  44.3 195.4 %all-gather.4.cloned.1.call-start = ((), (), s32[]{:S(2)}) async-start(), calls=%async_computation.3 | async-start | bytes 17301504 | tf_op jit(solution)/shard_map/all_gather | solution.py:145
  94.4 5.8 %copy-start.13 = (f32[18,6]{0,1:T(8,128)S(1)}, f32[18,6]{0,1:T(8,128)}, u32[]{:S(2)}) copy-start(f32[18,6]{0,1:T(8,128)} %param.37) | copy-start | bytes 1300
  96.7 34.5 %all-to-all-start.1 = ((bf16[32,6,2048]{2,1,0:T(8,128)(2,1)}), bf16[32,6,2048]{2,1,0:T(8,128)(2,1)S(1)}, u32[]{:S(2)}, u32[]{:S(2)}) async-start(bf16[32,6,2048]{2,1,0:T(8,128)(2,1)} %reshape.284), calls=%async_computation.1 | async-start | bytes 2097152 | tf_op jit(solution)/shard_map/all_to_all | solution.py:125
  100.3 22.8 %copy-start.5 = (bf16[2048,128]{1,0:T(8,128)(2,1)S(1)}, bf16[2048,128]{1,0:T(8,128)(2,1)}, u32[]{:S(2)}) copy-start(bf16[2048,128]{1,0:T(8,128)(2,1)} %param.41) | copy-start | bytes 1572868
  123.1 2.6 %copy-start.3 = (bf16[576,2048]{1,0:T(8,128)(2,1)S(1)}, bf16[576,2048]{1,0:T(8,128)(2,1)}, u32[]{:S(2)}) copy-start(bf16[576,2048]{1,0:T(8,128)(2,1)} %reshape.299) | copy-start | bytes 7077892
  123.1 2.6 %copy-start.14 = (bf16[2048,128]{1,0:T(8,128)(2,1)S(1)}, bf16[2048,128]{1,0:T(8,128)(2,1)}, u32[]{:S(2)}) copy-start(bf16[2048,128]{1,0:T(8,128)(2,1)} %param.42) | copy-start | bytes 1572868
  131.1 16.9 %all-to-all-start.2 = ((bf16[32,18,128]{2,1,0:T(8,128)(2,1)}), bf16[32,18,128]{2,1,0:T(8,128)(2,1)S(1)}, u32[]{:S(2)}, u32[]{:S(2)}) async-start(bf16[32,18,128]{2,1,0:T(8,128)(2,1)} %all_to_all.18), calls=%async_computation.2 | async-start | bytes 393216 | tf_op jit(solution)/shard_map/all_to_all | solution.py:138
  135.2 104.6 %copy-start.9 = (f32[4096]{0:T(1024)S(1)}, f32[4096]{0:T(1024)}, u32[]{:S(2)}) copy-start(f32[4096]{0:T(1024)} %param.44) | copy-start | bytes 49156
  239.8 8.9 %copy-start.1 = (bf16[1,512,2048]{2,1,0:T(8,128)(2,1)S(1)}, bf16[1,512,2048]{2,1,0:T(8,128)(2,1)}, u32[]{:S(2)}) copy-start(bf16[1,512,2048]{2,1,0:T(8,128)(2,1)} %param.40) | copy-start | bytes 6291460
Sparse Core Ops, SparseCore 0:
  44.5 74.2 all-gather.5
  121.6 118.1 all-gather.3
where the time goes:
time: 256 us
  waiting for transfers between devices  126 us (49%)
  blocking collectives  37.9 us (15%)
  matrix products  32.6 us (13%)
  local copies, waits for them, and re-layouts  31.9 us (12%)
  between operations  13.8 us (5%)
  starting transfers between devices  7.36 us (3%)
  other arithmetic  5.48 us (2%)
    all_gather x1, waiting for transfers between devices, shards(): lax.all_gather(w_dense_down, 'ep', axis=0, tiled=True)  91.2 us
    all_to_all x1, blocking collectives, shards(): lax.all_to_all(outgoing, 'ep', split_axis=0, concat_axis=0, tiled=True)  37.9 us
    all_gather x1, waiting for transfers between devices, shards(): piece = lax.all_gather(routed_in, 'ep', axis=0, tiled=True)  18.4 us
    unnamed x43, local copies, waits for them, and re-layouts  18.2 us
    all_to_all x1, waiting for transfers between devices, shards(): lax.all_to_all(units, 'ep', split_axis=0, concat_axis=1, tiled=True)  12.2 us
    dot_general x1, matrix products, shards(): jnp.dot(hidden, lax.all_gather(w_dense_down, 'ep', axis=0, tiled=True), p...  8.89 us
    gather x5, local copies, waits for them, and re-layouts, attend(): jnp.take_along_axis(cache_logcum, last_index, axis=2)[:, :, 0] + log_forget  5.84 us
  transfers between devices with their start and end apart: 4, of which 4 were waited for; matrix products, arithmetic and copies ran while one was open for 9% of the time, Pallas kernels for 0%

commit v1 on v0

--- a/solution.py
+++ b/solution.py
@@ -54,6 +54,15 @@
     return out.reshape(seqs, HEADS * HEAD_DIM).astype(jnp.bfloat16)
 
 
+def split3(values):
+    parts = []
+    for _ in range(3):
+        part = stored(values)
+        parts.append(part)
+        values = values - part.astype(jnp.float32)
+    return parts
+
+
 def expert_unit(rows, gate_w, up_w, down_w):
     gate = jnp.minimum(jnp.dot(rows, gate_w, preferred_element_type=jnp.float32), LIMIT)
     up = jnp.clip(jnp.dot(rows, up_w, preferred_element_type=jnp.float32), -LIMIT, LIMIT)
@@ -103,52 +112,49 @@
     )
     routed_in = normalize(mixed.astype(jnp.float32), expert_norm_gain).astype(jnp.bfloat16)
     devices = lax.axis_size("ep")
-    experts = devices * w_expert_gate.shape[0]
-    capacity = max(2, 2 * seqs * TOPK // experts)
-    flat_ids = expert_ids.reshape(-1)
-    member = (flat_ids[:, None] == jnp.arange(experts, dtype=jnp.int32)[None, :]).astype(jnp.int32)
-    slot = jnp.sum(jnp.cumsum(member, axis=0) * member, axis=1) - 1
-    target = flat_ids * capacity + slot
-    placement = (
-        target[:, None] == jnp.arange(experts * capacity, dtype=jnp.int32)[None, :]
-    ).astype(jnp.float32)
-    per_token = jnp.sum(placement.reshape(seqs, TOPK, experts * capacity), axis=1).astype(
+    me = lax.axis_index("ep")
+    capacity = max(2, 2 * seqs * TOPK // devices)
+    extra = jnp.concatenate(
+        [expert_ids.astype(jnp.bfloat16), *split3(expert_weights)], axis=1
+    )
+    packed = jnp.concatenate([routed_in, jnp.pad(extra, ((0, 0), (0, 128 - 4 * TOPK)))], axis=1)
+    everyone = lax.all_gather(packed, "ep", axis=0, tiled=True)
+    piece = everyone[:, :width]
+    side = everyone[:, width:].astype(jnp.float32)
+    ids_all = side[:, :TOPK].astype(jnp.int32)
+    weights_all = (
+        side[:, TOPK : 2 * TOPK] + side[:, 2 * TOPK : 3 * TOPK] + side[:, 3 * TOPK : 4 * TOPK]
+    )
+    gate_dense = jnp.dot(piece, w_dense_gate, preferred_element_type=jnp.float32)
+    up_dense = jnp.dot(piece, w_dense_up, preferred_element_type=jnp.float32)
+    units = stored(jax.nn.silu(gate_dense) * up_dense).astype(jnp.float32)
+    squares = lax.psum(jnp.sum(units * units, axis=1), "ep")
+    named = ids_all == me
+    mine = jnp.sum(jnp.where(named, weights_all, 0.0), axis=1)
+    member = jnp.any(named, axis=1).reshape(devices, seqs)
+    order = jnp.cumsum(member.astype(jnp.int32), axis=1) - 1
+    row = (order + capacity * jnp.arange(devices, dtype=jnp.int32)[:, None]).reshape(-1)
+    row = jnp.where(member.reshape(-1), row, -1)
+    choose = (row[:, None] == jnp.arange(devices * capacity, dtype=jnp.int32)[None, :]).astype(
         jnp.bfloat16
     )
-    outgoing = jnp.einsum("sc,sd->cd", per_token, routed_in, preferred_element_type=jnp.float32)
-    outgoing = outgoing.astype(jnp.bfloat16).reshape(experts, capacity, width)
-    arrived = lax.all_to_all(outgoing, "ep", split_axis=0, concat_axis=0, tiled=True)
-    count = arrived.shape[1]
-    answer = expert_unit(
-        arrived.reshape(-1, width), w_expert_gate[0], w_expert_up[0], w_expert_down[0]
+    arrived = lax.dot_general(
+        choose, piece, (((0,), (0,)), ((), ())), preferred_element_type=jnp.float32
+    ).astype(jnp.bfloat16)
+    answer = expert_unit(arrived, w_expert_gate[0], w_expert_up[0], w_expert_down[0])
+    routed = mine[:, None] * jnp.dot(choose, answer, preferred_element_type=jnp.float32)
+    units_total = dense_norm_gain.shape[0]
+    local = units.shape[1]
+    unit_scale = lax.rsqrt(squares / units_total + EPS)
+    gain = lax.dynamic_slice_in_dim(dense_norm_gain, me * local, local, 0)
+    hidden = (units * unit_scale[:, None] * gain).astype(jnp.bfloat16)
+    dense = jnp.dot(hidden, w_dense_down, preferred_element_type=jnp.float32)
+    branch_scale = jax.nn.sigmoid(
+        jnp.sum(piece.astype(jnp.float32) * branch_gate, axis=1, keepdims=True)
     )
-    returned = lax.all_to_all(
-        answer.reshape(devices, count, width), "ep", split_axis=0, concat_axis=0, tiled=True
-    )
-    picked = jnp.dot(
-        placement.astype(jnp.bfloat16),
-        returned.reshape(experts * capacity, width),
-        preferred_element_type=jnp.float32,
-    )
-    routed = jnp.sum(expert_weights[:, :, None] * picked.reshape(seqs, TOPK, width), axis=1)
-    piece = lax.all_gather(routed_in, "ep", axis=0, tiled=True)
-    gate_dense = jnp.dot(piece, w_dense_gate, preferred_element_type=jnp.float32)
-    up_dense = jnp.dot(piece, w_dense_up, preferred_element_type=jnp.float32)
-    units = (jax.nn.silu(gate_dense) * up_dense).astype(jnp.bfloat16)
-    own_units = lax.all_to_all(units, "ep", split_axis=0, concat_axis=1, tiled=True).astype(
-        jnp.float32
-    )
-    unit_scale = lax.rsqrt(jnp.mean(own_units * own_units, axis=1, keepdims=True) + EPS)
-    hidden = (own_units * unit_scale * dense_norm_gain).astype(jnp.bfloat16)
-    dense = jnp.dot(
-        hidden,
-        lax.all_gather(w_dense_down, "ep", axis=0, tiled=True),
-        preferred_element_type=jnp.float32,
-    )
-    branch_scale = jax.nn.sigmoid(
-        jnp.sum(routed_in.astype(jnp.float32) * branch_gate, axis=1, keepdims=True)
-    )
-    return (mixed.astype(jnp.float32) + routed + branch_scale * dense).astype(jnp.bfloat16)
+    partial = (routed + branch_scale * dense).astype(jnp.bfloat16)
+    total = lax.psum_scatter(partial, "ep", scatter_dimension=0, tiled=True)
+    return (mixed.astype(jnp.float32) + total.astype(jnp.float32)).astype(jnp.bfloat16)
 
 
 def solution(mesh):

time: 256 us -> 294 us (1.15)
  blocking collectives: 37.9 us -> 120 us
  waiting for transfers between devices: 126 us -> 62 us
  starting transfers between devices: 7.36 us -> 19.9 us
  other arithmetic: 5.48 us -> 13.3 us
  matrix products: 32.6 us -> 27.4 us
    unnamed x0 -> x1, blocking collectives: none -> 81.9 us
    all_gather x2 -> x1, waiting for transfers between devices: 110 us -> 61.8 us  [shards(): everyone = lax.all_gather(packed, 'ep', axis=0, tiled=True)]
    psum x0 -> x1, blocking collectives: none -> 38.3 us  [shards(): squares = lax.psum(jnp.sum(units * units, axis=1), 'ep')]
    all_to_all x1 -> x0, blocking collectives: 37.9 us -> none  [shards(): lax.all_to_all(outgoing, 'ep', split_axis=0, concat_axis=0, tiled=True)]
    unnamed x0 -> x8, starting transfers between devices: none -> 19.9 us
    all_to_all x2 -> x0, waiting for transfers between devices: 16.1 us -> none  [the longest x1 12.2 us: shards(): lax.all_to_all(units, 'ep', split_axis=0, concat_axis=1, tiled=True)]
    unnamed x43 -> x44, local copies, waits for them, and re-layouts: 18.2 us -> 25.6 us
    all_to_all x2 -> x0, starting transfers between devices: 7.32 us -> none  [the longest x1 3.79 us: shards(): lax.all_to_all(units, 'ep', split_axis=0, concat_axis=1, tiled=True)]
  transfers between devices with their start and end apart: 4 -> 9, of which waited for: 4 -> 2; matrix products, arithmetic and copies ran while one was open for 9% -> 0% of each run, Pallas kernels for 0% -> 0%
where the time goes in v1:
time: 294 us; the launch traced here: 291 us
  blocking collectives  120 us (41%)
  waiting for transfers between devices  62 us (21%)
  local copies, waits for them, and re-layouts  34.1 us (12%)
  matrix products  27.4 us (9%)
  starting transfers between devices  19.9 us (7%)
  between operations  13.9 us (5%)
  other arithmetic  13.3 us (5%)
    unnamed x1, blocking collectives  81.9 us
    all_gather x1, waiting for transfers between devices, shards(): everyone = lax.all_gather(packed, 'ep', axis=0, tiled=True)  61.8 us
    psum x1, blocking collectives, shards(): squares = lax.psum(jnp.sum(units * units, axis=1), 'ep')  38.3 us
    unnamed x44, local copies, waits for them, and re-layouts  25.6 us
    unnamed x8, starting transfers between devices  19.9 us
  transfers between devices with their start and end apart: 9, of which 2 were waited for; matrix products, arithmetic and copies ran while one was open for 0% of the time, Pallas kernels for 0%

profile of v1, /device:TPU:0, one launch (start us, length us, event | category | flops | bytes accessed | tf_op | source)
XLA Modules:
  0.0 290.8 jit_solution(7933098534395926256)
XLA Ops:
  6.5 0.8 broadcast_compare_fusion
  7.3 0.7 broadcast_add_fusion
  8.0 0.7 iota_compare_fusion.4
  8.7 1.0 fusion.56
  9.8 0.7 convert_element_type.118
  10.5 0.7 convert_element_type.119
  11.2 0.7 fusion.76
  11.9 0.7 subtract_convert_fusion
  12.9 5.5 %gather_fusion = f32[144]{0:T(256)S(1)} fusion(f32[18,8,1024]{2,1,0:T(8,128)} %param.33, s32[144]{0:T(256)S(1)} %reshape.237), kind=kCustom, calls=%fused_computation | custom fusion | bytes 2880 | tf_op jit(solution)/shard_map/jit(take_along_axis)/gather | solution.py:37
  19.3 1.3 fusion.42
  20.7 2.0 convolution_convert_fusion.2
  22.8 0.9 broadcast_subtract_fusion
  23.8 1.2 reshape.230
  25.0 6.6 %copy.45 = bf16[18,1024,128]{1,2,0:T(8,128)(2,1)} copy(bf16[18,1024,128]{2,1,0:T(8,128)(2,1)} %param.31) | data formatting | bytes 9437184 | tf_op args[8]
  31.8 3.2 %fusion.83 = (f32[18,2,4]{2,1,0:T(2,128)S(1)}, f32[18,2,4,1024]{3,2,1,0:T(4,128)S(1)}) fusion(f32[18,2,4,1024]{3,2,1,0:T(4,128)S(1)} %reshape.230, bf16[18,2,4,64]{3,2,1,0:T(4,128)(2,1)S(1)} %reshape.228, bf16[18,1024,2,64]{1,3,2,0:T(8,128)(2,1)} %bitcast.50, pred[18,1024]{1,0:T(8,128)(4,1)S(1)} %iota_compare_fusion.4), kind=kOutput, calls=%fused_computation.111 | convolution fusion | flops 19464048 | bytes 5935680 | tf_op jit(solution)/shard_map/skgd,slkd->skgl/dot_general | solution.py:40
  35.0 0.4 fusion.44
  35.5 6.6 %copy.49 = bf16[18,1024,128]{1,2,0:T(8,128)(2,1)} copy(bf16[18,1024,128]{2,1,0:T(8,128)(2,1)} %param.32) | data formatting | bytes 9437184 | tf_op args[9]
  42.1 3.7 %fusion.41 = bf16[18,2,4,64]{3,2,1,0:T(4,128)(2,1)S(1)} fusion(bf16[18,1024,2,64]{1,3,2,0:T(8,128)(2,1)} %bitcast.51, f32[18,2,4,1024]{3,2,1,0:T(4,128)S(1)} %get-tuple-element.12, f32[18,2,4]{2,1,0:T(2,128)S(1)} %get-tuple-element.8, f32[18,2,4]{2,1,0:T(2,128)S(1)} %multiply_maximum_fusion, f32[18,2,64]{2,1,0:T(2,128)S(1)} %reshape.233, ...), kind=kOutput, calls=%fused_computation.30 | convolution fusion | flops 19344384 | bytes 5337792 | tf_op jit(solution)/shard_map/skgl,slkd->skgd/dot_general | solution.py:52
  45.9 2.0 fusion.1
  48.2 0.6 fusion.67
  48.9 0.8 dynamic_slice.3
  49.6 61.8 %all-gather.3.cloned.1.call-done = bf16[32,18,2176]{2,1,0:T(8,128)(2,1)} async-done(((bf16[1,18,2176]{2,1,0:T(8,128)(2,1)}), bf16[32,18,2176]{2,1,0:T(8,128)(2,1)}) %all-gather.3.cloned.1.call-update) | async-done | bytes 2506768 | tf_op jit(solution)/shard_map/all_gather | solution.py:121
  111.4 4.4 %reshape.246 = bf16[576,2176]{1,0:T(8,128)(2,1)} reshape(bf16[32,18,2176]{2,1,0:T(8,128)(2,1)} %all-gather.3.cloned.1.call-done) | data formatting | bytes 5013504
  115.8 1.1 slice_convert_fusion.1
  116.9 2.2 multiply_reduce_fusion
  119.2 1.9 fusion.9
  121.1 0.8 fusion.38
  122.0 38.3 %psum.7 = f32[576]{0:T(1024)S(1)} all-reduce(f32[576]{0:T(1024)S(1)} %fusion.45), channel_id=1, replica_groups=mesh['ep'=32] {'ep'}, use_global_device_ids=true, to_apply=%region_9.10 | all-reduce | flops 576 | bytes 4608 | tf_op jit(solution)/shard_map/psum | solution.py:131
  160.4 0.4 fusion.49
  161.5 2.7 convolution_convert_fusion.1
  164.2 0.6 fusion.29
  164.8 1.0 copy-done.14
  165.8 0.6 fusion.35
  166.4 3.3 %fusion.13 = f32[576,2048]{1,0:T(8,128)} fusion(bf16[192,512]{1,0:T(8,128)(2,1)S(1)} %fusion.35, bf16[1,512,2048]{2,1,0:T(8,128)(2,1)S(1)} %copy-done, s32[576]{0:T(1024)S(1)} %broadcast_select_fusion), kind=kOutput, calls=%fused_computation.17 | convolution fusion | flops 856141824 | bytes 7014656 | tf_op jit(solution)/shard_map/dot_general | solution.py:145
  169.8 4.6 %add_convert_fusion = bf16[576,2048]{1,0:T(8,128)(2,1)} fusion(f32[576,2048]{1,0:T(8,128)} %fusion.13, bf16[128,2048]{1,0:T(8,128)(2,1)S(1)} %copy-done.5, f32[576]{0:T(1024)S(1)} %add_divide_fusion, f32[576]{0:T(1024)S(1)} %get-tuple-element.5, bf16[576,128]{1,0:T(8,128)(2,1)S(1)} %fusion.38, f32[128]{0:T(128)S(1)} %dynamic_slice.3, f32[576]{0:T(1024)S(1)} %add_rsqrt_fusion), kind=kOutput, calls=%fused_computation.1 | convolution fusion | flops 307003392 | bytes 7757056 | tf_op jit(solution)/shard_map/dot_general | solution.py:151
  174.4 81.9 %fusion = bf16[24,2048]{1,0:T(8,128)(2,1)S(1)} fusion(bf16[576,2048]{1,0:T(8,128)(2,1)} %add_convert_fusion), kind=kCustom, calls=%all-reduce-scatter | all-reduce-scatter fusion | flops 1572865 | bytes 2457600
  256.3 1.3 collective-permute-start.6
  257.6 1.3 collective-permute-start.5
  258.9 1.3 collective-permute-start.7
  260.2 1.3 collective-permute-start.4
  261.6 2.3 collective-permute-start.3
  263.9 1.3 collective-permute-start.2
  265.2 9.2 %collective-permute-start.1 = (bf16[24,2048]{1,0:T(8,128)(2,1)S(1)}, bf16[24,2048]{1,0:T(8,128)(2,1)S(1)}, u32[]{:S(2)}, u32[]{:S(2)}) collective-permute-start(bf16[24,2048]{1,0:T(8,128)(2,1)S(1)} %fusion), channel_id=1, source_target_pairs={{0,2},{1,3},{2,4},{3,5},{4,6},{5,7},{6,8},{7,9},{8,10},{9,11},{10,... | collective-permute-start | bytes 294920
  274.4 1.9 collective-permute-start
  276.6 0.4 copy-done.7
  277.1 0.6 copy-done.10
  277.7 5.5 %concatenate.11 = bf16[210,2048]{1,0:T(8,128)(2,1)S(1)} concatenate(bf16[18,2048]{1,0:T(8,128)(2,1)S(1)} %collective-permute-done.7, bf16[24,2048]{1,0:T(8,128)(2,1)S(1)} %collective-permute-done.6, bf16[24,2048]{1,0:T(8,128)(2,1)S(1)} %collective-permute-done.5, bf16[24,2048]{1,0:T(8,128)(2,1)} %copy-done.7, bf16[24,2048]{1,0:T(8,128)(2,1)} %copy-done.8, ...), dimensions={0} | concatenate | bytes 1720320
  283.2 0.7 fusion.62
  (81 shorter events, 3.1 us)
Async XLA Ops:
  6.5 159.9 %copy-start = (bf16[1,512,2048]{2,1,0:T(8,128)(2,1)S(1)}, bf16[1,512,2048]{2,1,0:T(8,128)(2,1)}, u32[]{:S(2)}) copy-start(bf16[1,512,2048]{2,1,0:T(8,128)(2,1)} %param.40) | copy-start | bytes 6291460
  6.5 104.9 %all-gather.3.cloned.1.call-start = ((), (), s32[]{:S(2)}) async-start(), calls=%async_computation | async-start | bytes 3446784 | tf_op jit(solution)/shard_map/all_gather | solution.py:121
  12.9 5.7 %copy-start.3 = (bf16[18,2048]{1,0:T(8,128)(2,1)S(1)}, bf16[18,2048]{1,0:T(8,128)(2,1)}, u32[]{:S(2)}) copy-start(bf16[18,2048]{1,0:T(8,128)(2,1)} %param.23) | copy-start | bytes 221188
  12.9 5.7 %copy-start.6 = (bf16[2048,128]{1,0:T(8,128)(2,1)S(1)}, bf16[2048,128]{1,0:T(8,128)(2,1)}, u32[]{:S(2)}) copy-start(bf16[2048,128]{1,0:T(8,128)(2,1)} %param.26) | copy-start | bytes 1572868
  12.9 5.7 %copy-start.11 = (f32[2048]{0:T(1024)S(1)}, f32[2048]{0:T(1024)}, u32[]{:S(2)}) copy-start(f32[2048]{0:T(1024)} %param.24) | copy-start | bytes 24580
  12.9 6.0 %copy-start.16 = (bf16[2048,8]{0,1:T(8,128)(2,1)S(1)}, bf16[2048,8]{0,1:T(8,128)(2,1)}, u32[]{:S(2)}) copy-start(bf16[2048,8]{0,1:T(8,128)(2,1)} %param.28) | copy-start | bytes 98308
  12.9 6.0 %copy-start.17 = (f32[8]{0:T(128)S(1)}, f32[8]{0:T(128)}, u32[]{:S(2)}) copy-start(f32[8]{0:T(128)} %param.29) | copy-start | bytes 100
  18.5 4.4 %copy-start.1 = (f32[18,8,1024]{2,1,0:T(8,128)S(1)}, f32[18,8,1024]{2,1,0:T(8,128)}, u32[]{:S(2)}) copy-start(f32[18,8,1024]{2,1,0:T(8,128)} %param.33) | copy-start | bytes 1769476
  42.1 6.0 %copy-start.13 = (f32[2048]{0:T(1024)S(1)}, f32[2048]{0:T(1024)}, u32[]{:S(2)}) copy-start(f32[2048]{0:T(1024)} %param.35) | copy-start | bytes 24580
  49.6 67.3 %copy-start.12 = (f32[2048]{0:T(1024)S(1)}, f32[2048]{0:T(1024)}, u32[]{:S(2)}) copy-start(f32[2048]{0:T(1024)} %param.45) | copy-start | bytes 24580
  115.8 3.3 %copy-start.2 = (bf16[576,2176]{1,0:T(8,128)(2,1)S(1)}, bf16[576,2176]{1,0:T(8,128)(2,1)}, u32[]{:S(2)}) copy-start(bf16[576,2176]{1,0:T(8,128)(2,1)} %reshape.246) | copy-start | bytes 7520260
  119.2 1.9 copy-start.15
  161.4 2.7 copy-start.4
  164.2 1.6 copy-start.14
  166.4 3.3 %copy-start.5 = (bf16[128,2048]{1,0:T(8,128)(2,1)S(1)}, bf16[128,2048]{1,0:T(8,128)(2,1)}, u32[]{:S(2)}) copy-start(bf16[128,2048]{1,0:T(8,128)(2,1)} %param.43) | copy-start | bytes 1572868
  256.3 8.9 %collective-permute-start.6 = (bf16[24,2048]{1,0:T(8,128)(2,1)S(1)}, bf16[24,2048]{1,0:T(8,128)(2,1)S(1)}, u32[]{:S(2)}, u32[]{:S(2)}) collective-permute-start(bf16[24,2048]{1,0:T(8,128)(2,1)S(1)} %fusion), channel_id=1, source_target_pairs={{0,7},{1,8},{2,9},{3,10},{4,11},{5,12},{6,13},{7,14},{8,15},{9,16}... | collective-permute-start | bytes 294920
  257.6 16.8 %collective-permute-start.5 = (bf16[24,2048]{1,0:T(8,128)(2,1)S(1)}, bf16[24,2048]{1,0:T(8,128)(2,1)S(1)}, u32[]{:S(2)}, u32[]{:S(2)}) collective-permute-start(bf16[24,2048]{1,0:T(8,128)(2,1)S(1)} %fusion), channel_id=1, source_target_pairs={{0,6},{1,7},{2,8},{3,9},{4,10},{5,11},{6,12},{7,13},{8,14},{9,15},... | collective-permute-start | bytes 294920
  258.9 4.9 %collective-permute-start.7 = (bf16[18,2048]{1,0:T(8,128)(2,1)S(1)}, bf16[18,2048]{1,0:T(8,128)(2,1)S(1)}, u32[]{:S(2)}, u32[]{:S(2)}) collective-permute-start(bf16[18,2048]{1,0:T(8,128)(2,1)S(1)} %slice.36), channel_id=1, source_target_pairs={{0,8},{1,9},{2,10},{3,11},{4,12},{5,13},{6,14},{7,15},{8,16},{9,17... | collective-permute-start | bytes 221192
  260.2 16.1 %collective-permute-start.4 = (bf16[24,2048]{1,0:T(8,128)(2,1)S(1)}, bf16[24,2048]{1,0:T(8,128)(2,1)S(1)}, u32[]{:S(2)}, u32[]{:S(2)}) collective-permute-start(bf16[24,2048]{1,0:T(8,128)(2,1)S(1)} %fusion), channel_id=1, source_target_pairs={{0,5},{1,6},{2,7},{3,8},{4,9},{5,10},{6,11},{7,12},{8,13},{9,14},{... | collective-permute-start | bytes 294920
  261.6 14.8 %collective-permute-start.3 = (bf16[24,2048]{1,0:T(8,128)(2,1)S(1)}, bf16[24,2048]{1,0:T(8,128)(2,1)S(1)}, u32[]{:S(2)}, u32[]{:S(2)}) collective-permute-start(bf16[24,2048]{1,0:T(8,128)(2,1)S(1)} %fusion), channel_id=1, source_target_pairs={{0,4},{1,5},{2,6},{3,7},{4,8},{5,9},{6,10},{7,11},{8,12},{9,13},{1... | collective-permute-start | bytes 294920
  263.9 12.5 %collective-permute-start.2 = (bf16[24,2048]{1,0:T(8,128)(2,1)S(1)}, bf16[24,2048]{1,0:T(8,128)(2,1)S(1)}, u32[]{:S(2)}, u32[]{:S(2)}) collective-permute-start(bf16[24,2048]{1,0:T(8,128)(2,1)S(1)} %fusion), channel_id=1, source_target_pairs={{0,3},{1,4},{2,5},{3,6},{4,7},{5,8},{6,9},{7,10},{8,11},{9,12},{10... | collective-permute-start | bytes 294920
  265.2 11.4 %collective-permute-start.1 = (bf16[24,2048]{1,0:T(8,128)(2,1)S(1)}, bf16[24,2048]{1,0:T(8,128)(2,1)S(1)}, u32[]{:S(2)}, u32[]{:S(2)}) collective-permute-start(bf16[24,2048]{1,0:T(8,128)(2,1)S(1)} %fusion), channel_id=1, source_target_pairs={{0,2},{1,3},{2,4},{3,5},{4,6},{5,7},{6,8},{7,9},{8,10},{9,11},{10,... | collective-permute-start | bytes 294920
  274.4 3.3 %collective-permute-start = (bf16[24,2048]{1,0:T(8,128)(2,1)S(1)}, bf16[24,2048]{1,0:T(8,128)(2,1)}, u32[]{:S(2)}, u32[]{:S(2)}) collective-permute-start(bf16[24,2048]{1,0:T(8,128)(2,1)S(1)} %fusion), channel_id=1, source_target_pairs={{0,1},{1,2},{2,3},{3,4},{4,5},{5,6},{6,7},{7,8},{8,9},{9,10},{10,1... | collective-permute-start | bytes 294920
  276.3 0.6 copy-start.7
  276.4 0.7 copy-start.8
  276.4 0.7 copy-start.9
  277.1 0.6 copy-start.10
Sparse Core Ops, SparseCore 0:
  49.0 62.3 all-gather.2

commit v2 on v1

v2 whole, which is shorter than its diff:
```python
import functools

import jax
import jax.numpy as jnp
from jax import lax
from jax.experimental import pallas as pl
from jax.experimental.pallas import tpu as pltpu
from jax.sharding import PartitionSpec as P

HEADS = 8
KV_HEADS = 2
HEAD_DIM = 64
TOPK = 6


EPS = 1e-06
LIMIT = 7.0
ALPHA = 1.702


def normalize(values, gain):
    return values * lax.rsqrt(jnp.mean(values * values, axis=-1, keepdims=True) + EPS) * gain


def stored(values):
    return lax.optimization_barrier(values.astype(jnp.bfloat16))


def front_body(
    lengths,
    tokens,
    gain_ref,
    w_query,
    w_key,
    w_value,
    w_forget,
    bias,
    w_out,
    gain_next,
    keys,
    values,
    logcum,
    mixed_ref,
    routed_ref,
    query_s,
    key_s,
    value_s,
    forget_s,
    attended_s,
):
    step = pl.program_id(0)
    batch, length, pair = keys.shape
    rows = jnp.float32
    group = HEADS // KV_HEADS
    tiles = HEADS * HEAD_DIM // pair

    @pl.when(step == 0)
    def _():
        normed = normalize(tokens[...].astype(rows), gain_ref[...]).astype(jnp.bfloat16)
        for weight, kept in ((w_key, key_s), (w_value, value_s)):
            product = jnp.dot(normed, weight[...], preferred_element_type=rows)
            kept[...] = product.astype(jnp.bfloat16).astype(rows)
        product = jnp.dot(normed, w_query[...], preferred_element_type=rows)
        product = product.astype(jnp.bfloat16).astype(rows)
        for tile in range(tiles):
            query_s[tile] = product[:, tile * pair : (tile + 1) * pair]
        forget = lax.dot_general(
            w_forget[...], normed, (((1,), (1,)), ((), ())), preferred_element_type=rows
        )
        forget = forget + bias[...]
        forget_s[...] = jnp.minimum(forget, 0.0) - jnp.log1p(jnp.exp(-jnp.abs(forget)))

    lane = lax.broadcasted_iota(jnp.int32, (HEADS, pair), 1)
    head = lax.broadcasted_iota(jnp.int32, (HEADS, pair), 0)
    odd = lane // HEAD_DIM
    place = head // group
    seq_lane = lax.broadcasted_iota(jnp.int32, forget_s.shape, 1)
    position = lax.broadcasted_iota(jnp.int32, (HEADS, length), 1)
    scale = HEAD_DIM ** (-0.5)
    for item in range(batch):
        seq = step * batch + item
        stay = jnp.zeros((HEADS, pair), rows)
        move = jnp.zeros((HEADS, pair), rows)
        for tile in range(tiles):
            piece = jnp.broadcast_to(
                query_s[tile, pl.ds(seq, 1), :], (HEADS, pair)
            )
            own_lanes = head == 2 * tile + odd
            stay = jnp.where(own_lanes & (odd == place), piece, stay)
            move = jnp.where(own_lanes & (odd != place), piece, move)
        query = stay + pltpu.roll(move, HEAD_DIM, 1)
        own = jnp.sum(query * key_s[pl.ds(seq, 1), :], axis=1, keepdims=True) * scale
        forget = jnp.sum(jnp.where(seq_lane == seq, forget_s[...], 0.0), axis=1, keepdims=True)
        cum = logcum[item]
        live_count = lengths[seq]
        last = jnp.sum(jnp.where(position == live_count - 1, cum, 0.0), axis=1, keepdims=True)
        scores = lax.dot_general(
            query.astype(jnp.bfloat16),
            keys[item],
            (((1,), (1,)), ((), ())),
            preferred_element_type=rows,
        )
        scores = scores * scale + ((last + forget) - cum)
        scores = jnp.where(position < live_count, scores, -jnp.inf)
        top = jnp.maximum(jnp.max(scores, axis=1, keepdims=True), own)
        expo = jnp.exp(scores - top)
        own_expo = jnp.exp(own - top)
        total = jnp.sum(expo, axis=1, keepdims=True) + own_expo
        weights = (expo / total).astype(jnp.bfloat16)
        own_weight = (own_expo / total).astype(jnp.bfloat16).astype(rows)
        out = jnp.dot(weights, values[item], preferred_element_type=rows)
        out = out + own_weight * value_s[pl.ds(seq, 1), :]
        turned = pltpu.roll(out, HEAD_DIM, 1)
        for tile in range(tiles):
            own_lanes = head == 2 * tile + odd
            part = jnp.where(own_lanes, jnp.where(odd == place, out, turned), 0.0)
            attended_s[tile, pl.ds(seq, 1), :] = jnp.sum(part, axis=0, keepdims=True)

    @pl.when(step == pl.num_programs(0) - 1)
    def _():
        attended = jnp.concatenate([attended_s[tile] for tile in range(tiles)], axis=1)
        attended = attended.astype(jnp.bfloat16)
        mixed = tokens[...].astype(rows) + jnp.dot(
            attended, w_out[...], preferred_element_type=rows
        )
        mixed = mixed.astype(jnp.bfloat16)
        mixed_ref[...] = mixed
        routed_ref[...] = normalize(mixed.astype(rows), gain_next[...]).astype(jnp.bfloat16)


def front(
    tokens, gain, w_query, w_key, w_value, w_forget, bias, w_out, keys, values, logcum, lengths, gain_next
):
    seqs, width = tokens.shape
    batch = max(size for size in (1, 2, 3) if seqs % size == 0)
    pair = keys.shape[2]

    def whole(*shape):
        return pl.BlockSpec(shape, lambda i, *_: (0,) * len(shape))

    def each(*shape):
        return pl.BlockSpec((batch, *shape), lambda i, *_: (i, 0, 0))

    small = (
        tokens,
        gain[None, :],
        w_query,
        w_key,
        w_value,
        w_forget.T,
        bias[:, None],
        w_out,
        gain_next[None, :],
    )
    kept = jax.ShapeDtypeStruct((seqs, width), jnp.bfloat16)
    return pl.pallas_call(
        front_body,
        out_shape=(kept, kept),
        grid_spec=pltpu.PrefetchScalarGridSpec(
            num_scalar_prefetch=1,
            grid=(seqs // batch,),
            in_specs=[whole(*array.shape) for array in small]
            + [each(*keys.shape[1:]), each(*values.shape[1:]), each(*logcum.shape[1:])],
            out_specs=[whole(seqs, width)] * 2,
            scratch_shapes=[
                pltpu.VMEM((HEADS * HEAD_DIM // pair, seqs, pair), jnp.float32),
                pltpu.VMEM((seqs, pair), jnp.float32),
                pltpu.VMEM((seqs, pair), jnp.float32),
                pltpu.VMEM((HEADS, seqs), jnp.float32),
                pltpu.VMEM((HEADS * HEAD_DIM // pair, seqs, pair), jnp.float32),
            ],
        ),
        compiler_params=pltpu.CompilerParams(
            dimension_semantics=("arbitrary",), vmem_limit_bytes=40 * 1024 * 1024
        ),
        cost_estimate=pl.CostEstimate(
            flops=10**9, bytes_accessed=16 * 10**6, transcendentals=2 * 10**5
        ),
        name="front",
    )(lengths, *small, keys, values, logcum)


def split3(values):
    parts = []
    for _ in range(3):
        part = stored(values)
        parts.append(part)
        values = values - part.astype(jnp.float32)
    return parts


def expert_unit(rows, gate_w, up_w, down_w):
    gate = jnp.minimum(jnp.dot(rows, gate_w, preferred_element_type=jnp.float32), LIMIT)
    up = jnp.clip(jnp.dot(rows, up_w, preferred_element_type=jnp.float32), -LIMIT, LIMIT)
    act = ((up + 1.0) * gate * jax.nn.sigmoid(gate * ALPHA)).astype(jnp.bfloat16)
    return jnp.dot(act, down_w, preferred_element_type=jnp.float32).astype(jnp.bfloat16)


def reach(source, target, sent, landed, device):
    return pltpu.make_async_remote_copy(
        src_ref=source,
        dst_ref=target,
        send_sem=sent,
        recv_sem=landed,
        device_id=(device,),
        device_id_type=pl.DeviceIdType.MESH,
    )


def to_row(column, same):
    return jnp.sum(jnp.where(same, column, 0.0), axis=0, keepdims=True)


def to_column(row, same):
    return jnp.sum(jnp.where(same, row, 0.0), axis=1, keepdims=True)


def rest_body(
    units_total,
    packed,
    mixed,
    w_gate,
    w_up,
    w_down,
    d_gate,
    d_up,
    d_down,
    gain,
    branch,
    out,
    rows_s,
    units_s,
    answer_s,
    coef_s,
    square_s,
    squares_s,
    theirs_s,
    joint_s,
    final_s,
    own_sem,
    ag_send,
    ag_recv,
    fw_send,
    fw_recv,
    sq_send,
    sq_recv,
    d2d_send,
    d2d_recv,
    rs_send,
    rs_recv,
):
    kind = jnp.float32
    n = squares_s.shape[0]
    chips = n // 2
    pad = packed.shape[0]
    width = out.shape[1]
    chunk = units_s.shape[1] // pad
    halves = chips // chunk
    size = chunk * pad
    me = lax.axis_index("ep")
    core = lax.rem(me, 2)
    chip = me // 2
    other = chip * 2 + 1 - core
    mine = core * chips
    peer = (1 - core) * chips

    barrier = pltpu.get_barrier_semaphore()

    @pl.loop(1, n)
    def _(k):
        pl.semaphore_signal(
            barrier,
            inc=1,
            device_id=(lax.rem(me + k, n),),
            device_id_type=pl.DeviceIdType.MESH,
        )

    pl.semaphore_wait(barrier, n - 1)

    def ahead(k):
        return lax.rem(chip + k, chips)

    def behind(k):
        return lax.rem(chip - k + chips, chips)

    def gather(k):
        return reach(
            packed, rows_s.at[mine + chip], ag_send.at[k], ag_recv.at[k], ahead(k) * 2 + core
        )

    def landed(k):
        slot = rows_s.at[mine + behind(k)]
        return reach(packed, slot, ag_send.at[k], ag_recv.at[k], behind(k) * 2 + core)

    def forward(k):
        slot = rows_s.at[mine + behind(k)]
        return reach(slot, slot, fw_send.at[k], fw_recv.at[k], other)

    def forwarded(k):
        slot = rows_s.at[peer + behind(k)]
        return reach(slot, slot, fw_send.at[k], fw_recv.at[k], other)

    keep = pltpu.make_async_copy(packed, rows_s.at[mine + chip], own_sem)
    keep.start()

    @pl.loop(1, chips)
    def _(k):
        gather(k).start()

    keep.wait()
    forward(0).start()

    @pl.loop(1, chips)
    def _(k):
        landed(k).wait_recv()
        forward(k).start()

    @pl.loop(0, chips)
    def _(k):
        forwarded(k).wait_recv()

    first = lax.broadcasted_iota(jnp.int32, (size, size), 0)
    second = lax.broadcasted_iota(jnp.int32, (size, size), 1)
    same = first == second

    def load(at):
        block = rows_s[pl.ds(at * chunk, chunk)]
        return block.astype(kind).reshape(size, block.shape[2])

    @pl.loop(0, 2 * halves)
    def _(at):
        wide = load(at)
        block = wide[:, :width].astype(jnp.bfloat16)
        gate = jnp.dot(block, d_gate[...], preferred_element_type=kind)
        up = jnp.dot(block, d_up[...], preferred_element_type=kind)
        units = (gate * jax.nn.sigmoid(gate) * up).astype(jnp.bfloat16).astype(kind)
        units_s[at] = units
        square_s[at] = to_row(jnp.sum(units * units, axis=1, keepdims=True), same)
        side = wide[:, width:]
        lane = lax.broadcasted_iota(jnp.int32, side.shape, 1)
        picked = jnp.where((side == me.astype(kind)) & (lane < TOPK), 1.0, 0.0)
        weight = jnp.zeros((size, 1), kind)
        for part in (3, 2, 1):
            moved = pltpu.roll(side, side.shape[1] - part * TOPK, 1)
            weight = weight + jnp.sum(picked * moved, axis=1, keepdims=True)
        branch_scale = jax.nn.sigmoid(
            jnp.sum(wide[:, :width] * branch[...], axis=1, keepdims=True)
        )
        coef_s[at] = jnp.where(lane == 0, weight, branch_scale)

    def share(k):
        return reach(
            square_s, squares_s.at[k], sq_send.at[k], sq_recv.at[k], lax.rem(me + k, n)
        )

    @pl.loop(1, n)
    def _(k):
        share(k).start()

    @pl.loop(0, 2 * halves)
    def _(at):
        block = load(at)[:, :width].astype(jnp.bfloat16)
        answer_s[at] = expert_unit(block, w_gate[...], w_up[...], w_down[...])

    @pl.loop(1, n)
    def _(k):
        share(k).wait_recv()

    squares_s[0] = square_s[...]
    totals = jnp.sum(squares_s[...], axis=0)
    square_rows = lax.rsqrt(totals / units_total + EPS)
    squares_s[0] = square_rows

    def partial(at):
        scale = to_column(squares_s[0, at], same)
        hidden = (units_s[at] * scale * gain[...]).astype(jnp.bfloat16)
        dense = jnp.dot(hidden, d_down[...], preferred_element_type=kind)
        coef = coef_s[at]
        routed = coef[:, 0:1] * answer_s[at].astype(kind)
        return (routed + coef[:, 1:2] * dense).reshape(chunk, pad, width)

    def cross(half):
        part = pl.ds(half * chunk, chunk)
        return reach(theirs_s.at[part], joint_s.at[part], d2d_send.at[half], d2d_recv.at[half], other)

    def back(k):
        to = behind(k)
        return reach(joint_s.at[to], final_s.at[k], rs_send.at[k], rs_recv.at[k], to * 2 + core)

    @pl.loop(0, halves)
    def _(half):
        theirs_s[pl.ds(half * chunk, chunk)] = partial((1 - core) * halves + half).astype(
            jnp.bfloat16
        )
        cross(half).start()

    @pl.loop(0, halves)
    def _(half):
        part = pl.ds(half * chunk, chunk)
        own = partial(core * halves + half)
        cross(half).wait_recv()
        joint_s[part] = (own + joint_s[part].astype(kind)).astype(jnp.bfloat16)

    @pl.loop(1, chips)
    def _(k):
        back(k).start()

    @pl.loop(1, chips)
    def _(k):
        back(k).wait_recv()

    total = joint_s[chip].astype(kind)
    for k in range(1, chips):
        total = total + final_s[k].astype(kind)
    result = mixed[...].astype(kind) + total[: mixed.shape[0]]
    out[...] = result.astype(jnp.bfloat16)

    @pl.loop(1, chips)
    def _(k):
        gather(k).wait_send()
        back(k).wait_send()

    @pl.loop(0, chips)
    def _(k):
        forward(k).wait_send()

    @pl.loop(1, n)
    def _(k):
        share(k).wait_send()

    @pl.loop(0, halves)
    def _(half):
        cross(half).wait_send()


def rest(n, packed, mixed, w_gate, w_up, w_down, d_gate, d_up, d_down, gain, branch, units_total):
    pad = packed.shape[0]
    width = mixed.shape[1]
    local = d_gate.shape[1]
    chips = n // 2
    chunk = max(size for size in (1, 2, 4, 8) if chips % size == 0)
    halves = chips // chunk
    size = chunk * pad
    half_type = jnp.bfloat16
    vmem = pl.BlockSpec(memory_space=pltpu.VMEM)
    dma = pltpu.SemaphoreType.DMA
    return pl.pallas_call(
        functools.partial(rest_body, units_total),
        out_shape=jax.ShapeDtypeStruct(mixed.shape, half_type),
        in_specs=[vmem] * 10,
        out_specs=vmem,
        scratch_shapes=[
            pltpu.VMEM((n, *packed.shape), half_type),
            pltpu.VMEM((2 * halves, size, local), jnp.float32),
            pltpu.VMEM((2 * halves, size, width), half_type),
            pltpu.VMEM((2 * halves, size, 128), jnp.float32),
            pltpu.VMEM((2 * halves, 1, size), jnp.float32),
            pltpu.VMEM((n, 2 * halves, 1, size), jnp.float32),
            pltpu.VMEM((chips, pad, width), half_type),
            pltpu.VMEM((chips, pad, width), half_type),
            pltpu.VMEM((chips, pad, width), half_type),
            dma,
            dma((chips,)),
            dma((chips,)),
            dma((chips,)),
            dma((chips,)),
            dma((n,)),
            dma((n,)),
            dma((halves,)),
            dma((halves,)),
            dma((chips,)),
            dma((chips,)),
        ],
        compiler_params=pltpu.CompilerParams(
            collective_id=0, has_side_effects=True, vmem_limit_bytes=62 * 1024 * 1024
        ),
        name="rest",
    )(packed, mixed, w_gate, w_up, w_down, d_gate, d_up, d_down, gain, branch)


def shards(
    tokens,
    attn_norm_gain,
    w_query,
    w_key,
    w_value,
    w_forget,
    forget_bias,
    w_attn_out,
    cache_keys,
    cache_values,
    cache_logcum,
    cache_lengths,
    expert_norm_gain,
    expert_ids,
    expert_weights,
    w_expert_gate,
    w_expert_up,
    w_expert_down,
    w_dense_gate,
    w_dense_up,
    w_dense_down,
    dense_norm_gain,
    branch_gate,
):
    mixed, routed_in = front(
        tokens,
        attn_norm_gain,
        w_query,
        w_key,
        w_value,
        w_forget,
        forget_bias,
        w_attn_out,
        cache_keys,
        cache_values,
        cache_logcum,
        cache_lengths,
        expert_norm_gain,
    )
    n = lax.axis_size("ep")
    me = lax.axis_index("ep")
    seqs = tokens.shape[0]
    extra = jnp.concatenate([expert_ids.astype(jnp.bfloat16), *split3(expert_weights)], axis=1)
    packed = jnp.concatenate([routed_in, jnp.pad(extra, ((0, 0), (0, 128 - 4 * TOPK)))], axis=1)
    packed = jnp.pad(packed, ((0, -seqs % 8), (0, 0)))
    local = w_dense_gate.shape[1]
    gain = lax.dynamic_slice_in_dim(dense_norm_gain, me * local, local, 0)
    return rest(
        n,
        packed,
        mixed,
        w_expert_gate[0],
        w_expert_up[0],
        w_expert_down[0],
        w_dense_gate,
        w_dense_up,
        w_dense_down,
        gain[None, :],
        branch_gate[None, :],
        dense_norm_gain.shape[0],
    )


def solution(mesh):
    in_specs = (
        P("ep", None),
        P(),
        P(),
        P(),
        P(),
        P(),
        P(),
        P(),
        P("ep", None, None),
        P("ep", None, None),
        P("ep", None, None),
        P("ep"),
        P(),
        P("ep", None),
        P("ep", None),
        P("ep", None, None),
        P("ep", None, None),
        P("ep", None, None),
        P(None, "ep"),
        P(None, "ep"),
        P("ep", None),
        P(),
        P(),
    )
    out_specs = P("ep", None)
    return jax.shard_map(shards, mesh=mesh, in_specs=in_specs, out_specs=out_specs, check_vma=False)
```

time: 294 us -> 138 us (0.47)
  blocking collectives: 120 us -> 0 us
  Pallas kernels: 0 us -> 118 us
  waiting for transfers between devices: 62 us -> 0 us
  matrix products: 27.4 us -> 0 us
  starting transfers between devices: 19.9 us -> 0 us
  local copies, waits for them, and re-layouts: 34.1 us -> 16.9 us
  between operations: 13.9 us -> 0.04 us
  other arithmetic: 13.3 us -> 2.14 us
    pallas_call x0 -> x2, Pallas kernels: none -> 118 us  [the longest x1 107 us: rest(): pl.pallas_call(functools.partial(rest_body, units_total), out_shape=jax.S...]
    unnamed x1 -> x0, blocking collectives: 81.9 us -> none
    all_gather x1 -> x0, waiting for transfers between devices: 61.8 us -> none  [shards(): everyone = lax.all_gather(packed, 'ep', axis=0, tiled=True)]
    psum x1 -> x0, blocking collectives: 38.3 us -> none  [shards(): squares = lax.psum(jnp.sum(units * units, axis=1), 'ep')]
    dot_general x15 -> x0, matrix products: 27.4 us -> none  [the longest x1 4.61 us: shards(): dense = jnp.dot(hidden, w_dense_down, preferred_element_type=jnp.float32)]
    unnamed x8 -> x0, starting transfers between devices: 19.9 us -> none
    unnamed x44 -> x28, local copies, waits for them, and re-layouts: 25.6 us -> 15.3 us
    gather x5 -> x0, local copies, waits for them, and re-layouts: 5.83 us -> none  [attend(): jnp.take_along_axis(cache_logcum, last_index, axis=2)[:, :, 0] + log_forget]
  transfers between devices with their start and end apart: 9 -> 0, of which waited for: 2 -> 0; matrix products, arithmetic and copies ran while one was open for 0% -> 0% of each run, Pallas kernels for 0% -> 0%
where the time goes in v2:
time: 138 us; the launch traced here: 137 us
  Pallas kernels  118 us (86%)
  local copies, waits for them, and re-layouts  16.9 us (12%)
  other arithmetic  2.14 us (2%)
    pallas_call x1, Pallas kernels, rest(): pl.pallas_call(functools.partial(rest_body, units_total), out_shape=jax.S...  107 us
    unnamed x28, local copies, waits for them, and re-layouts  15.3 us
    pallas_call x1, Pallas kernels, front(): pl.pallas_call(front_body, out_shape=(kept, kept), grid_spec=pltpu.Prefet...  11.4 us

profile of v2, /device:TPU:0, one launch (start us, length us, event | category | flops | bytes accessed | tf_op | source)
XLA Modules:
  0.0 137.4 jit_solution(14480285683301653210)
XLA Ops:
  0.0 0.0 copy-start
  0.0 0.7 convert_element_type.23
  0.7 0.1 copy.32
  0.8 0.8 copy.30
  1.6 0.7 convert_element_type.22
  2.3 0.1 copy.31
  2.4 0.1 fusion.10
  2.5 0.7 copy.28.bias
  3.2 0.0 copy-start.1
  3.2 2.3 %copy-done.1 = bf16[18,1024,128]{2,1,0:T(8,128)(2,1)S(1)} copy-done((bf16[18,1024,128]{2,1,0:T(8,128)(2,1)S(1)}, bf16[18,1024,128]{2,1,0:T(8,128)(2,1)}, u32[]{:S(2)}) %copy-start.1) | copy-done | bytes 4718616
  5.6 0.0 copy-start.2
  5.6 1.6 %copy-done.2 = bf16[2048,512]{1,0:T(8,128)(2,1)S(1)} copy-done((bf16[2048,512]{1,0:T(8,128)(2,1)S(1)}, bf16[2048,512]{1,0:T(8,128)(2,1)}, u32[]{:S(2)}) %copy-start.2) | copy-done | bytes 2097176
  7.2 0.0 copy-start.3
  7.2 1.6 %copy-done.3 = bf16[512,2048]{1,0:T(8,128)(2,1)S(1)} copy-done((bf16[512,2048]{1,0:T(8,128)(2,1)S(1)}, bf16[512,2048]{1,0:T(8,128)(2,1)}, u32[]{:S(2)}) %copy-start.3) | copy-done | bytes 2097176
  8.8 0.0 copy-start.4
  8.8 1.1 copy-done.4
  9.8 0.0 copy-start.5
  9.8 1.0 copy-done.5
  10.9 0.0 copy-start.6
  10.9 1.0 copy-done.6
  11.9 0.0 copy-start.7
  11.9 0.9 copy-done.7
  12.8 0.0 copy-start.9
  12.8 0.8 copy-done.9
  13.6 0.0 copy-start.10
  13.6 0.7 copy-done.10
  14.3 0.0 copy-start.11
  14.3 0.7 copy-done.11
  15.0 0.0 copy-start.12
  15.0 0.7 copy-done.12
  15.6 11.4 %front.1 = (bf16[18,2048]{1,0:T(8,128)(2,1)S(1)}, bf16[18,2048]{1,0:T(8,128)(2,1)S(1)}) custom-call(s32[18]{0:T(128)S(1)} %copy-done.12, bf16[18,2048]{1,0:T(8,128)(2,1)S(1)} %copy-done.7, f32[1,2048]{1,0:T(1,128)S(1)} %bitcast.11, bf16[2048,512]{1,0:T(8,128)(2,1)S(1)} %copy-done.2, bf16[2048,128]{1,0:T(8,128)(2,1)S(1)} %copy-done.5, ...), custom_call_target="tpu_custom_call" | custom-call | flops 1000000000 | bytes 16000000 | tf_op jit(solution)/shard_map/front/pallas_call | solution.py:156
  27.0 0.0 copy-start.8
  27.0 0.6 copy-done.8
  27.6 0.6 fusion.2.packed
  28.3 0.0 copy-done
  28.3 0.6 dynamic-slice_bitcast_fusion.gain
  28.9 106.9 %rest.1 = bf16[18,2048]{1,0:T(8,128)(2,1)} custom-call(bf16[24,2176]{1,0:T(8,128)(2,1)} %fusion.2.packed, bf16[18,2048]{1,0:T(8,128)(2,1)} %copy-done.8, bf16[2048,512]{1,0:T(8,128)(2,1)} %bitcast.13, bf16[2048,512]{1,0:T(8,128)(2,1)} %bitcast.14, bf16[512,2048]{1,0:T(8,128)(2,1)} %bitcast.15, bf16[2048,128]{1,0:T(8,128)(2,1)} %d_gate.1, ...), custom_call_target="tpu_custom_call" | custom-call | tf_op jit(solution)/shard_map/rest/pallas_call | solution.py:447
  135.8 1.5 %copy.34 = bf16[18,2048]{1,0:T(8,128)(2,1)} copy(bf16[18,2048]{1,0:T(8,128)(2,1)} %rest.1) | data formatting | bytes 147456
  (2 shorter events, 0.0 us)
Async XLA Ops:
  0.0 28.3 %copy-start = (f32[4096]{0:T(1024)S(1)}, f32[4096]{0:T(1024)}, u32[]{:S(2)}) copy-start(f32[4096]{0:T(1024)} %param.44) | copy-start | bytes 49156
  3.2 2.3 %copy-start.1 = (bf16[18,1024,128]{2,1,0:T(8,128)(2,1)S(1)}, bf16[18,1024,128]{2,1,0:T(8,128)(2,1)}, u32[]{:S(2)}) copy-start(bf16[18,1024,128]{2,1,0:T(8,128)(2,1)} %keys.1) | copy-start | bytes 14155780
  5.6 1.6 %copy-start.2 = (bf16[2048,512]{1,0:T(8,128)(2,1)S(1)}, bf16[2048,512]{1,0:T(8,128)(2,1)}, u32[]{:S(2)}) copy-start(bf16[2048,512]{1,0:T(8,128)(2,1)} %w_query.1) | copy-start | bytes 6291460
  7.2 1.6 %copy-start.3 = (bf16[512,2048]{1,0:T(8,128)(2,1)S(1)}, bf16[512,2048]{1,0:T(8,128)(2,1)}, u32[]{:S(2)}) copy-start(bf16[512,2048]{1,0:T(8,128)(2,1)} %w_out.1) | copy-start | bytes 6291460
  8.8 1.1 copy-start.4
  9.8 1.0 copy-start.5
  10.9 1.0 copy-start.6
  11.9 0.9 copy-start.7
  12.8 0.8 copy-start.9
  13.6 0.7 copy-start.10
  14.3 0.7 copy-start.11
  15.0 0.7 copy-start.12
  27.0 0.6 copy-start.8

commit v3 on v2

--- a/solution.py
+++ b/solution.py
@@ -217,6 +217,7 @@
 
 def rest_body(
     units_total,
+    plane,
     packed,
     mixed,
     w_gate,
@@ -277,47 +278,76 @@
 
     pl.semaphore_wait(barrier, n - 1)
 
-    def ahead(k):
-        return lax.rem(chip + k, chips)
-
-    def behind(k):
-        return lax.rem(chip - k + chips, chips)
-
-    def gather(k):
-        return reach(
-            packed, rows_s.at[mine + chip], ag_send.at[k], ag_recv.at[k], ahead(k) * 2 + core
-        )
-
-    def landed(k):
-        slot = rows_s.at[mine + behind(k)]
-        return reach(packed, slot, ag_send.at[k], ag_recv.at[k], behind(k) * 2 + core)
-
-    def forward(k):
-        slot = rows_s.at[mine + behind(k)]
+    deep = chips // plane
+    level = chip // plane
+    spot = lax.rem(chip, plane)
+
+    def before(dz, dp):
+        return lax.rem(level - dz + deep, deep) * plane + lax.rem(spot - dp + plane, plane)
+
+    def along(dz):
+        to = lax.rem(level + dz, deep) * plane + spot
+        k = dz * plane
+        return reach(packed, rows_s.at[mine + chip], ag_send.at[k], ag_recv.at[k], to * 2 + core)
+
+    def across(dz, dp):
+        to = level * plane + lax.rem(spot + dp, plane)
+        k = dz * plane + dp
+        slot = rows_s.at[mine + before(dz, 0)]
+        return reach(slot, slot, ag_send.at[k], ag_recv.at[k], to * 2 + core)
+
+    def landed(dz, dp):
+        slot = rows_s.at[mine + before(dz, dp)]
+        k = dz * plane + dp
+        return reach(slot, slot, ag_send.at[k], ag_recv.at[k], before(0, dp) * 2 + core)
+
+    def forward(dz, dp):
+        slot = rows_s.at[mine + before(dz, dp)]
+        k = dz * plane + dp
         return reach(slot, slot, fw_send.at[k], fw_recv.at[k], other)
 
-    def forwarded(k):
-        slot = rows_s.at[peer + behind(k)]
+    def forwarded(dz, dp):
+        slot = rows_s.at[peer + before(dz, dp)]
+        k = dz * plane + dp
         return reach(slot, slot, fw_send.at[k], fw_recv.at[k], other)
 
     keep = pltpu.make_async_copy(packed, rows_s.at[mine + chip], own_sem)
     keep.start()
 
-    @pl.loop(1, chips)
-    def _(k):
-        gather(k).start()
+    @pl.loop(1, deep)
+    def _(dz):
+        along(dz).start()
 
     keep.wait()
-    forward(0).start()
-
-    @pl.loop(1, chips)
-    def _(k):
-        landed(k).wait_recv()
-        forward(k).start()
-
-    @pl.loop(0, chips)
-    def _(k):
-        forwarded(k).wait_recv()
+
+    @pl.loop(1, plane)
+    def _(dp):
+        across(0, dp).start()
+
+    forward(0, 0).start()
+
+    @pl.loop(1, deep)
+    def _(dz):
+        landed(dz, 0).wait_recv()
+
+        @pl.loop(1, plane)
+        def _(dp):
+            across(dz, dp).start()
+
+        forward(dz, 0).start()
+
+    @pl.loop(0, deep)
+    def _(dz):
+        @pl.loop(1, plane)
+        def _(dp):
+            landed(dz, dp).wait_recv()
+            forward(dz, dp).start()
+
+    @pl.loop(0, deep)
+    def _(dz):
+        @pl.loop(0, plane)
+        def _(dp):
+            forwarded(dz, dp).wait_recv()
 
     first = lax.broadcasted_iota(jnp.int32, (size, size), 0)
     second = lax.broadcasted_iota(jnp.int32, (size, size), 1)
@@ -383,9 +413,22 @@
         part = pl.ds(half * chunk, chunk)
         return reach(theirs_s.at[part], joint_s.at[part], d2d_send.at[half], d2d_recv.at[half], other)
 
-    def back(k):
-        to = behind(k)
+    def back(dz, dp):
+        k = dz * plane + dp
+        slot = joint_s.at[before(dz, dp)]
+        return reach(slot, final_s.at[k], rs_send.at[k], rs_recv.at[k], before(0, dp) * 2 + core)
+
+    def down(dz):
+        k = dz * plane
+        to = before(dz, 0)
         return reach(joint_s.at[to], final_s.at[k], rs_send.at[k], rs_recv.at[k], to * 2 + core)
+
+    def collected(dz):
+        total = joint_s[before(dz, 0)].astype(kind)
+        for dp in range(1, plane):
+            back(dz, dp).wait_recv()
+            total = total + final_s[dz * plane + dp].astype(kind)
+        return total
 
     @pl.loop(0, halves)
     def _(half):
@@ -401,28 +444,38 @@
         cross(half).wait_recv()
         joint_s[part] = (own + joint_s[part].astype(kind)).astype(jnp.bfloat16)
 
-    @pl.loop(1, chips)
-    def _(k):
-        back(k).start()
-
-    @pl.loop(1, chips)
-    def _(k):
-        back(k).wait_recv()
-
-    total = joint_s[chip].astype(kind)
-    for k in range(1, chips):
-        total = total + final_s[k].astype(kind)
+    @pl.loop(1, deep + 1)
+    def _(step):
+        @pl.loop(1, plane)
+        def _(dp):
+            back(lax.rem(step, deep), dp).start()
+
+    @pl.loop(1, deep)
+    def _(dz):
+        joint_s[before(dz, 0)] = collected(dz).astype(jnp.bfloat16)
+        down(dz).start()
+
+    total = collected(0)
+    for dz in range(1, deep):
+        down(dz).wait_recv()
+        total = total + final_s[dz * plane].astype(kind)
     result = mixed[...].astype(kind) + total[: mixed.shape[0]]
     out[...] = result.astype(jnp.bfloat16)
 
-    @pl.loop(1, chips)
-    def _(k):
-        gather(k).wait_send()
-        back(k).wait_send()
-
-    @pl.loop(0, chips)
-    def _(k):
-        forward(k).wait_send()
+    @pl.loop(1, deep)
+    def _(dz):
+        along(dz).wait_send()
+        down(dz).wait_send()
+
+    @pl.loop(0, deep)
+    def _(dz):
+        forward(dz, 0).wait_send()
+
+        @pl.loop(1, plane)
+        def _(dp):
+            across(dz, dp).wait_send()
+            back(dz, dp).wait_send()
+            forward(dz, dp).wait_send()
 
     @pl.loop(1, n)
     def _(k):
@@ -440,12 +493,13 @@
     chips = n // 2
     chunk = max(size for size in (1, 2, 4, 8) if chips % size == 0)
     halves = chips // chunk
+    plane = chips // 4 if chips % 4 == 0 else chips
     size = chunk * pad
     half_type = jnp.bfloat16
     vmem = pl.BlockSpec(memory_space=pltpu.VMEM)
     dma = pltpu.SemaphoreType.DMA
     return pl.pallas_call(
-        functools.partial(rest_body, units_total),
+        functools.partial(rest_body, units_total, plane),
         out_shape=jax.ShapeDtypeStruct(mixed.shape, half_type),
         in_specs=[vmem] * 10,
         out_specs=vmem,

time: 138 us -> 100 us (0.72)
  Pallas kernels: 118 us -> 80.5 us
    pallas_call x1, Pallas kernels: 107 us -> 69.2 us  [rest(): pl.pallas_call(functools.partial(rest_body, units_total, plane), out_shap...]
where the time goes in v3:
time: 100 us; the launch traced here: 99.6 us
  Pallas kernels  80.5 us (80%)
  local copies, waits for them, and re-layouts  16.9 us (17%)
  other arithmetic  2.14 us (2%)
    pallas_call x1, Pallas kernels, rest(): pl.pallas_call(functools.partial(rest_body, units_total, plane), out_shap...  69.2 us
    unnamed x28, local copies, waits for them, and re-layouts  15.3 us
    pallas_call x1, Pallas kernels, front(): pl.pallas_call(front_body, out_shape=(kept, kept), grid_spec=pltpu.Prefet...  11.4 us

profile of v3, /device:TPU:0, one launch (start us, length us, event | category | flops | bytes accessed | tf_op | source)
XLA Modules:
  0.0 99.6 jit_solution(5491594527085155684)
XLA Ops:
  0.0 0.0 copy-start
  0.0 0.7 convert_element_type.23
  0.7 0.1 copy.32
  0.8 0.8 copy.30
  1.6 0.7 convert_element_type.22
  2.3 0.1 copy.31
  2.4 0.1 fusion.10
  2.5 0.7 copy.28.bias
  3.2 0.0 copy-start.1
  3.2 2.3 %copy-done.1 = bf16[18,1024,128]{2,1,0:T(8,128)(2,1)S(1)} copy-done((bf16[18,1024,128]{2,1,0:T(8,128)(2,1)S(1)}, bf16[18,1024,128]{2,1,0:T(8,128)(2,1)}, u32[]{:S(2)}) %copy-start.1) | copy-done | bytes 4718616
  5.6 0.0 copy-start.2
  5.6 1.6 %copy-done.2 = bf16[2048,512]{1,0:T(8,128)(2,1)S(1)} copy-done((bf16[2048,512]{1,0:T(8,128)(2,1)S(1)}, bf16[2048,512]{1,0:T(8,128)(2,1)}, u32[]{:S(2)}) %copy-start.2) | copy-done | bytes 2097176
  7.2 0.0 copy-start.3
  7.2 1.6 %copy-done.3 = bf16[512,2048]{1,0:T(8,128)(2,1)S(1)} copy-done((bf16[512,2048]{1,0:T(8,128)(2,1)S(1)}, bf16[512,2048]{1,0:T(8,128)(2,1)}, u32[]{:S(2)}) %copy-start.3) | copy-done | bytes 2097176
  8.8 0.0 copy-start.4
  8.8 1.1 %copy-done.4 = f32[18,8,1024]{2,1,0:T(8,128)S(1)} copy-done((f32[18,8,1024]{2,1,0:T(8,128)S(1)}, f32[18,8,1024]{2,1,0:T(8,128)}, u32[]{:S(2)}) %copy-start.4) | copy-done | bytes 589848
  9.8 0.0 copy-start.5
  9.8 1.0 %copy-done.5 = bf16[2048,128]{1,0:T(8,128)(2,1)S(1)} copy-done((bf16[2048,128]{1,0:T(8,128)(2,1)S(1)}, bf16[2048,128]{1,0:T(8,128)(2,1)}, u32[]{:S(2)}) %copy-start.5) | copy-done | bytes 524312
  10.9 0.0 copy-start.6
  10.9 1.0 %copy-done.6 = bf16[2048,128]{1,0:T(8,128)(2,1)S(1)} copy-done((bf16[2048,128]{1,0:T(8,128)(2,1)S(1)}, bf16[2048,128]{1,0:T(8,128)(2,1)}, u32[]{:S(2)}) %copy-start.6) | copy-done | bytes 524312
  11.9 0.0 copy-start.7
  11.9 0.9 copy-done.7
  12.8 0.0 copy-start.9
  12.8 0.8 copy-done.9
  13.6 0.0 copy-start.10
  13.6 0.7 copy-done.10
  14.3 0.0 copy-start.11
  14.3 0.7 copy-done.11
  15.0 0.0 copy-start.12
  15.0 0.7 copy-done.12
  15.6 11.4 %front.1 = (bf16[18,2048]{1,0:T(8,128)(2,1)S(1)}, bf16[18,2048]{1,0:T(8,128)(2,1)S(1)}) custom-call(s32[18]{0:T(128)S(1)} %copy-done.12, bf16[18,2048]{1,0:T(8,128)(2,1)S(1)} %copy-done.7, f32[1,2048]{1,0:T(1,128)S(1)} %bitcast.11, bf16[2048,512]{1,0:T(8,128)(2,1)S(1)} %copy-done.2, bf16[2048,128]{1,0:T(8,128)(2,1)S(1)} %copy-done.5, ...), custom_call_target="tpu_custom_call" | custom-call | flops 1000000000 | bytes 16000000 | tf_op jit(solution)/shard_map/front/pallas_call | solution.py:156
  27.0 0.0 copy-start.8
  27.0 0.6 copy-done.8
  27.6 0.6 fusion.2.packed
  28.3 0.0 copy-done
  28.3 0.6 dynamic-slice_bitcast_fusion.gain
  28.9 69.2 %rest.1 = bf16[18,2048]{1,0:T(8,128)(2,1)} custom-call(bf16[24,2176]{1,0:T(8,128)(2,1)} %fusion.2.packed, bf16[18,2048]{1,0:T(8,128)(2,1)} %copy-done.8, bf16[2048,512]{1,0:T(8,128)(2,1)} %bitcast.13, bf16[2048,512]{1,0:T(8,128)(2,1)} %bitcast.14, bf16[512,2048]{1,0:T(8,128)(2,1)} %bitcast.15, bf16[2048,128]{1,0:T(8,128)(2,1)} %d_gate.1, ...), custom_call_target="tpu_custom_call" | custom-call | tf_op jit(solution)/shard_map/rest/pallas_call | solution.py:501
  98.0 1.5 %copy.34 = bf16[18,2048]{1,0:T(8,128)(2,1)} copy(bf16[18,2048]{1,0:T(8,128)(2,1)} %rest.1) | data formatting | bytes 147456
  (2 shorter events, 0.0 us)
Async XLA Ops:
  0.0 28.3 %copy-start = (f32[4096]{0:T(1024)S(1)}, f32[4096]{0:T(1024)}, u32[]{:S(2)}) copy-start(f32[4096]{0:T(1024)} %param.44) | copy-start | bytes 49156
  3.2 2.3 %copy-start.1 = (bf16[18,1024,128]{2,1,0:T(8,128)(2,1)S(1)}, bf16[18,1024,128]{2,1,0:T(8,128)(2,1)}, u32[]{:S(2)}) copy-start(bf16[18,1024,128]{2,1,0:T(8,128)(2,1)} %keys.1) | copy-start | bytes 14155780
  5.6 1.6 %copy-start.2 = (bf16[2048,512]{1,0:T(8,128)(2,1)S(1)}, bf16[2048,512]{1,0:T(8,128)(2,1)}, u32[]{:S(2)}) copy-start(bf16[2048,512]{1,0:T(8,128)(2,1)} %w_query.1) | copy-start | bytes 6291460
  7.2 1.6 %copy-start.3 = (bf16[512,2048]{1,0:T(8,128)(2,1)S(1)}, bf16[512,2048]{1,0:T(8,128)(2,1)}, u32[]{:S(2)}) copy-start(bf16[512,2048]{1,0:T(8,128)(2,1)} %w_out.1) | copy-start | bytes 6291460
  8.8 1.1 %copy-start.4 = (f32[18,8,1024]{2,1,0:T(8,128)S(1)}, f32[18,8,1024]{2,1,0:T(8,128)}, u32[]{:S(2)}) copy-start(f32[18,8,1024]{2,1,0:T(8,128)} %logcum.1) | copy-start | bytes 1769476
  9.8 1.0 %copy-start.5 = (bf16[2048,128]{1,0:T(8,128)(2,1)S(1)}, bf16[2048,128]{1,0:T(8,128)(2,1)}, u32[]{:S(2)}) copy-start(bf16[2048,128]{1,0:T(8,128)(2,1)} %w_key.1) | copy-start | bytes 1572868
  10.9 1.0 %copy-start.6 = (bf16[2048,128]{1,0:T(8,128)(2,1)S(1)}, bf16[2048,128]{1,0:T(8,128)(2,1)}, u32[]{:S(2)}) copy-start(bf16[2048,128]{1,0:T(8,128)(2,1)} %w_value.1) | copy-start | bytes 1572868
  11.9 0.9 copy-start.7
  12.8 0.8 copy-start.9
  13.6 0.7 copy-start.10
  14.3 0.7 copy-start.11
  15.0 0.7 copy-start.12
  27.0 0.6 copy-start.8
